TPU v7x, 32 devices: a whole 2x2x4 slice. The times are simulated.
32 devices in a mesh: grp: 2 (over y), sp: 4 (over z), tp: 4 (over x, core).
Axes of the slice: x: 2, y: 2, z: 4, core: 2. Of those that a mesh axis runs over, the one named last changes fastest.
Arguments:
- queries_small: bfloat16 [2048, 1024], P(('grp', 'sp'), 'tp'), parts along dimension 0, may hold values from -6 to 6
- keys_small: bfloat16 [2048, 512], P(('grp', 'sp'), 'tp'), parts along dimension 0, may hold values from -6 to 6
- values_small: bfloat16 [2048, 512], P(('grp', 'sp'), 'tp'), parts along dimension 0, may hold values from -6 to 6
- queries_large: bfloat16 [2048, 1024], P(('grp', 'sp'), 'tp'), parts along dimension 0, may hold values from -6 to 6
- keys_large: bfloat16 [2048, 512], P(('grp', 'sp'), 'tp'), parts along dimension 0, may hold values from -6 to 6
- values_large: bfloat16 [2048, 512], P(('grp', 'sp'), 'tp'), parts along dimension 0, may hold values from -6 to 6
- query_gain_small: float32 [128], P('grp'), parts along dimension 0, may hold values from 1.2 to 12
- key_gain_small: float32 [128], P('grp'), parts along dimension 0, may hold values from 1.2 to 12
- query_gain_large: float32 [256], P('grp'), parts along dimension 0, may hold values from 1.2 to 12
- key_gain_large: float32 [256], P('grp'), parts along dimension 0, may hold values from 1.2 to 12
- residual_in: bfloat16 [2048, 2048], P(('grp', 'sp', 'tp')), parts along dimension 0, may hold values from -1.5 to 1.5
- out_weight_small: bfloat16 [1024, 2048], P('tp'), may hold values from -0.125 to 0.125
- out_weight_large: bfloat16 [1024, 2048], P('tp'), may hold values from -0.125 to 0.125
- norm_gain: float32 [2048], replicated, may hold values from 0.1 to 1.9
- routes: int32 [2048, 2], P(('grp', 'sp', 'tp')), parts along dimension 0, may hold values from 0 to 7, all different within a row; in each aligned block of 64 rows (0 to 63, 64 to 127, ...) at most 32 rows name the same one
- route_scores: float32 [2048, 2], P(('grp', 'sp', 'tp')), parts along dimension 0, may hold values from 0.05 to 1
- expert_gate: bfloat16 [8, 2048, 1024], P('sp', None, 'tp'), may hold values from -0.125 to 0.125
- expert_up: bfloat16 [8, 2048, 1024], P('sp', None, 'tp'), may hold values from -0.125 to 0.125
- expert_down: bfloat16 [8, 1024, 2048], P('sp', 'tp'), may hold values from -0.1875 to 0.1875
Outputs:
- result: bfloat16 [2048, 2048], P(('grp', 'sp', 'tp')), parts along dimension 0
There are 2 independent parts, one for each index of `grp`. A program takes and returns all parts, laid end to end along the dimension named above; an argument that names none is the same for every part. Nothing has to cross between parts.
Inputs may be any that keep to these rules, and one draw needn't show every extreme that they name: `routes`: each token names 2 different experts; within the rows of one device (aligned blocks of 64 tokens) no expert is named more than 32 times, a bound that some block reaches.
All inputs are finite; a program needn't handle non-finite values.
Results may differ from a plain program's by a relative error of at most 0.02.
The roundings to bfloat16 on the way count: a program that leaves them out, or rounds other values in their place, can miss the bound.
Values may be sent and summed in bfloat16 or wider, within the bound.
A program may use at most 128 MiB of HBM per device.

v0:
```python
import jax
import jax.numpy as jnp
from jax import lax
from jax.sharding import PartitionSpec as P

HS_SMALL = 64
HS_LARGE = 128
GRID_W = 64
theta_base = 10000.0
norm_eps = 1e-06
block_target = 1280


def grid_tables(offset, length, head_size):
    places = offset + jnp.arange(length, dtype=jnp.int32)
    grid_rows = (places // GRID_W).astype(jnp.float32)
    grid_cols = (places % GRID_W).astype(jnp.float32)
    rates = jnp.power(
        theta_base, -2.0 * jnp.arange(head_size // 4, dtype=jnp.float32) / (head_size // 2)
    )
    row_angles = grid_rows[:, None, None] * rates
    col_angles = grid_cols[:, None, None] * rates
    return (jnp.cos(row_angles), jnp.sin(row_angles), jnp.cos(col_angles), jnp.sin(col_angles))


def half_turn(segment, cosine, sine_part):
    half_size = segment.shape[-1] // 2
    leading = segment[..., :half_size]
    trailing = segment[..., half_size:]
    return jnp.concatenate(
        [leading * cosine - trailing * sine_part, trailing * cosine + leading * sine_part], axis=-1
    )


def grid_turn(vectors, tables):
    row_cos, row_sin, col_cos, col_sin = tables
    half_size = vectors.shape[-1] // 2
    return jnp.concatenate(
        [
            half_turn(vectors[..., :half_size], row_cos, row_sin),
            half_turn(vectors[..., half_size:], col_cos, col_sin),
        ],
        axis=-1,
    )


def normed_turn(raw_rows, gain, tables):
    widened = raw_rows.astype(jnp.float32)
    scaled = (
        widened * lax.rsqrt(jnp.mean(widened * widened, axis=-1, keepdims=True) + norm_eps) * gain
    )
    return grid_turn(scaled, tables).astype(jnp.bfloat16)


def block_rows(row_count, shard_rows):
    shards = row_count // shard_rows
    chosen = 1
    for factor in range(1, max(1, block_target // shard_rows) + 1):
        if shards % factor == 0:
            chosen = factor
    return chosen * shard_rows


def attend_block(state, queries, key_rows, value_rows):
    largest, weight_sum, accumulated = state
    head_size = queries.shape[-1]
    kv_local = queries.shape[1]
    key_heads = key_rows.reshape(key_rows.shape[0], kv_local, head_size)
    value_heads = value_rows.reshape(value_rows.shape[0], kv_local, head_size)
    scores = jnp.einsum(
        "qgrd,kgd->qgrk", queries, key_heads, preferred_element_type=jnp.float32
    ) * head_size ** (-0.5)
    peak_score = jnp.maximum(largest, jnp.max(scores, axis=-1))
    shrink = jnp.exp(largest - peak_score)
    weights = jnp.exp(scores - peak_score[..., None])
    weight_sum = weight_sum * shrink + jnp.sum(weights, axis=-1)
    accumulated = accumulated * shrink[..., None] + jnp.einsum(
        "qgrk,kgd->qgrd",
        weights.astype(jnp.bfloat16),
        value_heads,
        preferred_element_type=jnp.float32,
    )
    return (peak_score, weight_sum, accumulated)


def attend_rows(state, queries, key_rows, value_rows):
    row_count = key_rows.shape[0]
    step_rows = block_rows(row_count, queries.shape[0])
    if step_rows == row_count:
        return attend_block(state, queries, key_rows, value_rows)

    def one_block(block_index, carried):
        offset = block_index * step_rows
        return attend_block(
            carried,
            queries,
            lax.dynamic_slice_in_dim(key_rows, offset, step_rows, 0),
            lax.dynamic_slice_in_dim(value_rows, offset, step_rows, 0),
        )

    return lax.fori_loop(0, row_count // step_rows, one_block, state)


def empty_state(queries):
    state_shape = queries.shape[:3]
    return (
        jnp.full(state_shape, -1e30, jnp.float32),
        jnp.zeros(state_shape, jnp.float32),
        jnp.zeros(queries.shape, jnp.float32),
    )


def finish(state):
    largest, weight_sum, accumulated = state
    merged = accumulated / weight_sum[..., None]
    return merged.reshape(merged.shape[0], -1).astype(jnp.bfloat16)


def on_device(
    queries_small,
    keys_small,
    values_small,
    queries_large,
    keys_large,
    values_large,
    query_gain_small,
    key_gain_small,
    query_gain_large,
    key_gain_large,
    residual_in,
    out_weight_small,
    out_weight_large,
    norm_gain,
    routes,
    route_scores,
    expert_gate,
    expert_up,
    expert_down,
):
    token_rows = queries_small.shape[0]
    offset = lax.axis_index("sp") * token_rows
    tables_small = grid_tables(offset, token_rows, HS_SMALL)
    tables_large = grid_tables(offset, token_rows, HS_LARGE)
    kv_small = keys_small.shape[1] // HS_SMALL
    kv_large = keys_large.shape[1] // HS_LARGE
    asked_small = normed_turn(
        queries_small.reshape(token_rows, -1, HS_SMALL), query_gain_small, tables_small
    ).reshape(token_rows, kv_small, -1, HS_SMALL)
    asked_large = normed_turn(
        queries_large.reshape(token_rows, -1, HS_LARGE), query_gain_large, tables_large
    ).reshape(token_rows, kv_large, -1, HS_LARGE)
    turned_small = normed_turn(
        keys_small.reshape(token_rows, kv_small, HS_SMALL), key_gain_small, tables_small
    ).reshape(token_rows, -1)
    turned_large = normed_turn(
        keys_large.reshape(token_rows, kv_large, HS_LARGE), key_gain_large, tables_large
    ).reshape(token_rows, -1)
    key_small = lax.all_gather(turned_small, "sp", axis=0, tiled=True)
    value_small = lax.all_gather(values_small, "sp", axis=0, tiled=True)
    key_large = lax.all_gather(turned_large, "sp", axis=0, tiled=True)
    value_large = lax.all_gather(values_large, "sp", axis=0, tiled=True)
    state_small = attend_rows(empty_state(asked_small), asked_small, key_small, value_small)
    state_large = attend_rows(empty_state(asked_large), asked_large, key_large, value_large)
    heard_small = finish(state_small)
    heard_large = finish(state_large)
    projected = lax.psum_scatter(
        (
            jnp.dot(heard_small, out_weight_small, preferred_element_type=jnp.float32)
            + jnp.dot(heard_large, out_weight_large, preferred_element_type=jnp.float32)
        ).astype(jnp.bfloat16),
        "tp",
        scatter_dimension=0,
        tiled=True,
    ).astype(jnp.float32)
    attended = (residual_in.astype(jnp.float32) + projected).astype(jnp.bfloat16)
    widened = attended.astype(jnp.float32)
    normed = (
        widened
        * lax.rsqrt(jnp.mean(widened * widened, axis=-1, keepdims=True) + norm_eps)
        * norm_gain
    ).astype(jnp.bfloat16)
    local_rows = routes.shape[0]
    top_count = routes.shape[1]
    sp_count = lax.axis_size("sp")
    local_experts = expert_gate.shape[0]
    expert_count = local_experts * sp_count
    capacity = max(2, (2 * top_count * local_rows + expert_count - 1) // expert_count)
    flat_routes = routes.reshape(-1)
    member = (flat_routes[:, None] == jnp.arange(expert_count, dtype=jnp.int32)[None, :]).astype(
        jnp.int32
    )
    ranks = jnp.sum((jnp.cumsum(member, axis=0) - member) * member, axis=1)
    slots = flat_routes * capacity + ranks
    picker = (
        slots[:, None] == jnp.arange(expert_count * capacity, dtype=jnp.int32)[None, :]
    ).astype(jnp.bfloat16)
    placer = jnp.sum(picker.reshape(local_rows, top_count, -1), axis=1)
    outgoing = jnp.einsum("ts,td->sd", placer, normed, preferred_element_type=jnp.float32).astype(
        jnp.bfloat16
    )
    outgoing = outgoing.reshape(sp_count, local_experts, capacity, -1)
    everyone = lax.all_gather(
        lax.all_to_all(outgoing, "sp", split_axis=0, concat_axis=0, tiled=True),
        "tp",
        axis=0,
        tiled=True,
    )
    gate_out = jnp.einsum(
        "secd,edf->secf", everyone, expert_gate, preferred_element_type=jnp.float32
    )
    up_out = jnp.einsum("secd,edf->secf", everyone, expert_up, preferred_element_type=jnp.float32)
    active = (jax.nn.silu(gate_out) * up_out).astype(jnp.bfloat16)
    summed = lax.psum_scatter(
        jnp.einsum(
            "secf,efd->secd", active, expert_down, preferred_element_type=jnp.float32
        ).astype(jnp.bfloat16),
        "tp",
        scatter_dimension=0,
        tiled=True,
    )
    returned = lax.all_to_all(summed, "sp", split_axis=0, concat_axis=0, tiled=True)
    back_rows = returned.reshape(expert_count * capacity, -1)
    chosen_rows = jnp.dot(picker, back_rows, preferred_element_type=jnp.float32).reshape(
        local_rows, top_count, -1
    )
    shares = route_scores / jnp.sum(route_scores, axis=1, keepdims=True)
    mixed = jnp.sum(chosen_rows * shares[:, :, None], axis=1)
    return (attended.astype(jnp.float32) + mixed).astype(jnp.bfloat16)


def solution(mesh):
    in_specs = (
        P(("grp", "sp"), "tp"),
        P(("grp", "sp"), "tp"),
        P(("grp", "sp"), "tp"),
        P(("grp", "sp"), "tp"),
        P(("grp", "sp"), "tp"),
        P(("grp", "sp"), "tp"),
        P("grp"),
        P("grp"),
        P("grp"),
        P("grp"),
        P(("grp", "sp", "tp"), None),
        P("tp", None),
        P("tp", None),
        P(),
        P(("grp", "sp", "tp"), None),
        P(("grp", "sp", "tp"), None),
        P("sp", None, "tp"),
        P("sp", None, "tp"),
        P("sp", "tp", None),
    )
    out_specs = P(("grp", "sp", "tp"), None)
    return jax.shard_map(
        on_device, mesh=mesh, in_specs=in_specs, out_specs=out_specs, check_vma=False
    )
```

profile of v0, /device:TPU:0, one launch (start us, length us, event | category | flops | bytes accessed | tf_op | source)
XLA Modules:
  0.0 313.0 jit_solution(7394251430156797041)
XLA Ops:
  6.6 1.1 copy.83
  7.7 0.7 fusion.63
  8.5 1.0 multiply_cosine_fusion.1
  9.8 15.7 %all_gather.17 = bf16[1024,128]{0,1:T(8,128)(2,1)S(1)} all-gather(bf16[256,128]{0,1:T(8,128)(2,1)S(1)} %pad_maximum_fusion.1), channel_id=1, replica_groups=mesh['grp'=2,'sp'=4,'tp'=4] {'sp'}, dimensions={0}, use_global_device_ids=true | all-gather | bytes 327680 | tf_op jit(solution)/shard_map/all_gather | solution.py:160
  25.5 1.0 copy.84
  27.1 0.6 bitcast_reduce_fusion.1
  27.8 1.3 copy-done.2
  29.5 14.4 %all_gather.18 = bf16[1024,128]{0,1:T(8,128)(2,1)S(1)} all-gather(bf16[256,128]{0,1:T(8,128)(2,1)S(1)} %copy.87), channel_id=1, replica_groups=mesh['grp'=2,'sp'=4,'tp'=4] {'sp'}, dimensions={0}, use_global_device_ids=true | all-gather | bytes 327680 | tf_op jit(solution)/shard_map/all_gather | solution.py:161
  44.5 13.8 %all_gather.15 = bf16[1024,128]{0,1:T(8,128)(2,1)S(1)} all-gather(bf16[256,128]{0,1:T(8,128)(2,1)S(1)} %bitcast.168), channel_id=1, replica_groups=mesh['grp'=2,'sp'=4,'tp'=4] {'sp'}, dimensions={0}, use_global_device_ids=true | all-gather | bytes 327680 | tf_op jit(solution)/shard_map/all_gather | solution.py:158
  58.6 0.8 bitcast_reduce_fusion
  59.4 0.7 fusion.1
  60.1 1.2 copy-done.1
  61.3 13.8 %all_gather.16 = bf16[1024,128]{1,0:T(8,128)(2,1)S(1)} all-gather(bf16[256,128]{1,0:T(8,128)(2,1)S(1)} %copy-done.8), channel_id=1, replica_groups=mesh['grp'=2,'sp'=4,'tp'=4] {'sp'}, dimensions={0}, use_global_device_ids=true | all-gather | bytes 327680 | tf_op jit(solution)/shard_map/all_gather | solution.py:159
  75.3 3.1 fusion.38
  78.9 1.1 copy-done.3
  80.5 1.5 fusion.3
  83.1 25.4 %reduce-scatter.5.cloned.1.call-done = bf16[64,2048]{1,0:T(8,128)(2,1)} async-done(((bf16[256,2048]{1,0:T(8,128)(2,1)}), bf16[64,2048]{1,0:T(8,128)(2,1)}) %reduce-scatter.5.cloned.1.call-update) | async-done | bytes 262160 | tf_op jit(solution)/shard_map/reduce_scatter | solution.py:166
  108.5 1.1 fusion.48
  109.7 1.4 convolution_convert_fusion
  111.1 30.0 %all_to_all.10 = bf16[4,2,32,2048]{3,2,1,0:T(8,128)(2,1)S(1)} all-to-all(bf16[4,2,32,2048]{3,2,1,0:T(8,128)(2,1)S(1)} %bitcast.163), channel_id=1, replica_groups=mesh['grp'=2,'sp'=4,'tp'=4] {'sp'}, dimensions={0} | all-to-all | bytes 2097152 | tf_op jit(solution)/shard_map/all_to_all | solution.py:203
  141.1 1.0 copy.91
  142.4 32.5 %all-gather.2.cloned.1.call-done = bf16[16,2,32,2048]{3,2,0,1:T(8,128)(2,1)} async-done(((bf16[4,2,32,2048]{3,2,0,1:T(8,128)(2,1)}), bf16[16,2,32,2048]{3,2,0,1:T(8,128)(2,1)}) %all-gather.2.cloned.1.call-update) | async-done | bytes 4194320 | tf_op jit(solution)/shard_map/all_gather | solution.py:202
  174.9 4.1 %fusion.14 = f32[16,2,32,256]{3,2,0,1:T(8,128)S(1)} fusion(bf16[16,2,32,2048]{3,2,0,1:T(8,128)(2,1)} %all-gather.2.cloned.1.call-done, bf16[2,2048,256]{2,1,0:T(8,128)(2,1)} %param.35), kind=kOutput, calls=%fused_computation.21 | convolution fusion | flops 1073741824 | bytes 7340032 | tf_op jit(solution)/shard_map/secd,edf->secf/dot_general | solution.py:208
  179.0 7.3 %convert_bitcast_fusion = bf16[16,2,32,2048]{3,2,0,1:T(8,128)(2,1)} fusion(bf16[2,256,2048]{2,1,0:T(8,128)(2,1)S(1)} %copy-done, bf16[16,2,32,2048]{3,2,0,1:T(8,128)(2,1)} %all-gather.2.cloned.1.call-done, bf16[2,2048,256]{2,1,0:T(8,128)(2,1)} %param.36, f32[16,2,32,256]{3,2,0,1:T(8,128)S(1)} %fusion.14), kind=kOutput, calls=%fused_computation.3 | convolution fusion | flops 2151153664 | bytes 13631488 | tf_op jit(solution)/shard_map/secf,efd->secd/dot_general | solution.py:214
  186.3 0.6 copy-done.17
  187.0 0.6 dynamic-slice
  188.2 83.8 %all-reduce.3.cloned.1.call-done = bf16[16,2,32,2048]{3,2,0,1:T(8,128)(2,1)} async-done(((bf16[16,2,32,2048]{3,2,0,1:T(8,128)(2,1)}), bf16[16,2,32,2048]{3,2,0,1:T(8,128)(2,1)}) %all-reduce.3.cloned.1.call-update) | async-done | bytes 4194320
  272.0 1.3 constant_dynamic-slice_fusion
  273.3 1.1 copy.92
  274.4 4.6 %all-to-all-start.1 = ((bf16[4,2,32,2048]{3,2,1,0:T(8,128)(2,1)}), bf16[4,2,32,2048]{3,2,1,0:T(8,128)(2,1)S(1)}, u32[]{:S(2)}, u32[]{:S(2)}) async-start(bf16[4,2,32,2048]{3,2,1,0:T(8,128)(2,1)} %copy.92), calls=%async_computation.2 | async-start | bytes 2097152 | tf_op jit(solution)/shard_map/all_to_all | solution.py:221
  279.0 25.4 %all-to-all-done.1 = bf16[4,2,32,2048]{3,2,1,0:T(8,128)(2,1)S(1)} async-done(((bf16[4,2,32,2048]{3,2,1,0:T(8,128)(2,1)}), bf16[4,2,32,2048]{3,2,1,0:T(8,128)(2,1)S(1)}, u32[]{:S(2)}, u32[]{:S(2)}) %all-to-all-start.1) | async-done | bytes 1048608 | tf_op jit(solution)/shard_map/all_to_all | solution.py:221
  304.7 1.7 fusion.51
  (84 shorter events, 5.1 us)
Async XLA Ops:
  6.5 172.5 %copy-start = (bf16[2,256,2048]{2,1,0:T(8,128)(2,1)S(1)}, bf16[2,256,2048]{2,1,0:T(8,128)(2,1)}, u32[]{:S(2)}) copy-start(bf16[2,256,2048]{2,1,0:T(8,128)(2,1)} %param.37) | copy-start | bytes 6291460
  6.5 20.1 %copy-start.14 = (f32[128]{0:T(128)S(1)}, f32[128]{0:T(128)}, u32[]{:S(2)}) copy-start(f32[128]{0:T(128)} %param.27) | copy-start | bytes 1540
  6.5 102.0 %reduce-scatter.5.cloned.1.call-start = ((), (), s32[]{:S(2)}) async-start(), calls=%async_computation.3 | async-start | bytes 1310720 | tf_op jit(solution)/shard_map/reduce_scatter | solution.py:166
  27.1 2.4 copy-start.9
  27.1 17.1 %copy-start.10 = (bf16[256,128]{1,0:T(8,128)(2,1)S(1)}, bf16[256,128]{1,0:T(8,128)(2,1)}, u32[]{:S(2)}) copy-start(bf16[256,128]{1,0:T(8,128)(2,1)} %param.20) | copy-start | bytes 196612
  27.7 1.3 copy-start.2
  27.7 16.6 %copy-start.15 = (f32[64]{0:T(128)S(1)}, f32[64]{0:T(128)}, u32[]{:S(2)}) copy-start(f32[64]{0:T(128)} %param.26) | copy-start | bytes 772
  27.7 30.6 %copy-start.7 = (bf16[256,256]{1,0:T(8,128)(2,1)S(1)}, bf16[256,256]{1,0:T(8,128)(2,1)}, u32[]{:S(2)}) copy-start(bf16[256,256]{1,0:T(8,128)(2,1)} %param.19) | copy-start | bytes 393220
  27.7 30.7 %copy-start.16 = (f32[64]{0:T(128)S(1)}, f32[64]{0:T(128)}, u32[]{:S(2)}) copy-start(f32[64]{0:T(128)} %param.25) | copy-start | bytes 772
  59.4 1.9 copy-start.1
  59.4 1.9 copy-start.8
  75.3 3.1 copy-start.5
  78.4 1.6 copy-start.3
  78.9 1.6 copy-start.6
  80.5 1.6 copy-start.12
  80.5 28.0 %copy-start.4 = (bf16[64,2048]{1,0:T(8,128)(2,1)S(1)}, bf16[64,2048]{1,0:T(8,128)(2,1)}, u32[]{:S(2)}) copy-start(bf16[64,2048]{1,0:T(8,128)(2,1)} %param.29) | copy-start | bytes 786436
  80.5 29.1 %copy-start.11 = (f32[2048]{0:T(1024)S(1)}, f32[2048]{0:T(1024)}, u32[]{:S(2)}) copy-start(f32[2048]{0:T(1024)} %param.32) | copy-start | bytes 24580
  82.0 92.9 %all-gather.2.cloned.1.call-start = ((), (), s32[]{:S(2)}) async-start(), calls=%async_computation.4 | async-start | bytes 5242880 | tf_op jit(solution)/shard_map/all_gather | solution.py:202
  142.1 129.9 %all-reduce.3.cloned.1.call-start = ((), (), s32[]{:S(2)}) async-start(), calls=%async_computation.5 | async-start | bytes 8388608
  186.3 0.7 copy-start.17
  273.3 5.7 %copy-start.13 = (f32[64,2]{0,1:T(2,128)S(1)}, f32[64,2]{0,1:T(2,128)}, u32[]{:S(2)}) copy-start(f32[64,2]{0,1:T(2,128)} %param.34) | copy-start | bytes 1540
  274.4 30.0 %all-to-all-start.1 = ((bf16[4,2,32,2048]{3,2,1,0:T(8,128)(2,1)}), bf16[4,2,32,2048]{3,2,1,0:T(8,128)(2,1)S(1)}, u32[]{:S(2)}, u32[]{:S(2)}) async-start(bf16[4,2,32,2048]{3,2,1,0:T(8,128)(2,1)} %copy.92), calls=%async_computation.2 | async-start | bytes 2097152 | tf_op jit(solution)/shard_map/all_to_all | solution.py:221
Sparse Core Ops, SparseCore 0:
  82.1 26.3 reduce-scatter.4
  142.3 32.5 all-gather.1
  186.5 85.4 all-reduce.2
where the time goes:
time: 313 us
  waiting for transfers between devices  167 us (53%)
  blocking collectives  87.7 us (28%)
  matrix products  20.1 us (6%)
  between operations  14.3 us (5%)
  local copies, waits for them, and re-layouts  11.3 us (4%)
  other arithmetic  7.66 us (2%)
  starting transfers between devices  4.86 us (2%)
    unnamed x4, waiting for transfers between devices  83.8 us
    all_gather x1, waiting for transfers between devices, on_device(): lax.all_gather(lax.all_to_all(outgoing, 'sp', split_axis=0, concat_axis=0...  32.5 us
    all_to_all x1, blocking collectives, on_device(): lax.all_to_all(outgoing, 'sp', split_axis=0, concat_axis=0, tiled=True)  30 us
    reduce_scatter x1, waiting for transfers between devices, on_device(): lax.psum_scatter((jnp.dot(heard_small, out_weight_small, preferred_elemen...  25.4 us
    all_to_all x1, waiting for transfers between devices, on_device(): lax.all_to_all(summed, 'sp', split_axis=0, concat_axis=0, tiled=True)  25.4 us
    all_gather x1, blocking collectives, on_device(): key_large = lax.all_gather(turned_large, 'sp', axis=0, tiled=True)  15.7 us
    all_gather x1, blocking collectives, on_device(): value_large = lax.all_gather(values_large, 'sp', axis=0, tiled=True)  14.4 us
    all_gather x1, blocking collectives, on_device(): key_small = lax.all_gather(turned_small, 'sp', axis=0, tiled=True)  13.8 us
  transfers between devices with their start and end apart: 4, of which 4 were waited for; matrix products, arithmetic and copies ran while one was open for 1% of the time, Pallas kernels for 0%

commit v1 on v0

--- a/solution.py
+++ b/solution.py
@@ -156,8 +156,11 @@
         keys_large.reshape(token_rows, kv_large, HS_LARGE), key_gain_large, tables_large
     ).reshape(token_rows, -1)
     key_small = lax.all_gather(turned_small, "sp", axis=0, tiled=True)
-    value_small = lax.all_gather(values_small, "sp", axis=0, tiled=True)
-    key_large = lax.all_gather(turned_large, "sp", axis=0, tiled=True)
+    value_small, key_large = jnp.split(
+        lax.all_gather(jnp.concatenate([values_small, turned_large], 1), "sp", axis=0, tiled=True),
+        [values_small.shape[1]],
+        1,
+    )
     value_large = lax.all_gather(values_large, "sp", axis=0, tiled=True)
     state_small = attend_rows(empty_state(asked_small), asked_small, key_small, value_small)
     state_large = attend_rows(empty_state(asked_large), asked_large, key_large, value_large)

time: 313 us -> 303 us (0.968)
  blocking collectives: 87.7 us -> 75.8 us
    all_gather x2 -> x1, blocking collectives: 29.4 us -> 17.4 us  [on_device(): lax.all_gather(jnp.concatenate([values_small, turned_large], 1), 'sp', ax...]
    unnamed x44 -> x46, local copies, waits for them, and re-layouts: 8.64 us -> 8.67 us
where the time goes in v1:
time: 303 us
  waiting for transfers between devices  167 us (55%)
  blocking collectives  75.8 us (25%)
  matrix products  20.1 us (7%)
  between operations  14.3 us (5%)
  local copies, waits for them, and re-layouts  12.8 us (4%)
  other arithmetic  8.17 us (3%)
  starting transfers between devices  4.86 us (2%)
    unnamed x4, waiting for transfers between devices  83.8 us
    all_gather x1, waiting for transfers between devices, on_device(): lax.all_gather(lax.all_to_all(outgoing, 'sp', split_axis=0, concat_axis=0...  32.5 us
    all_to_all x1, blocking collectives, on_device(): lax.all_to_all(outgoing, 'sp', split_axis=0, concat_axis=0, tiled=True)  29.9 us
    all_to_all x1, waiting for transfers between devices, on_device(): lax.all_to_all(summed, 'sp', split_axis=0, concat_axis=0, tiled=True)  25.4 us
    reduce_scatter x1, waiting for transfers between devices, on_device(): lax.psum_scatter((jnp.dot(heard_small, out_weight_small, preferred_elemen...  25.2 us
    all_gather x1, blocking collectives, on_device(): lax.all_gather(jnp.concatenate([values_small, turned_large], 1), 'sp', ax...  17.4 us
    all_gather x1, blocking collectives, on_device(): value_large = lax.all_gather(values_large, 'sp', axis=0, tiled=True)  14.7 us
    all_gather x1, blocking collectives, on_device(): key_small = lax.all_gather(turned_small, 'sp', axis=0, tiled=True)  13.8 us
  transfers between devices with their start and end apart: 4, of which 4 were waited for; matrix products, arithmetic and copies ran while one was open for 1% of the time, Pallas kernels for 0%

profile of v1, /device:TPU:0, one launch (start us, length us, event | category | flops | bytes accessed | tf_op | source)
XLA Modules:
  0.0 302.9 jit_solution(11383160169731471180)
XLA Ops:
  7.1 1.0 copy.81
  8.1 0.7 fusion.62
  8.9 1.0 multiply_cosine_fusion.1
  10.7 1.0 concatenate.50
  11.7 17.4 %all_gather.13 = bf16[1024,256]{1,0:T(8,128)(2,1)S(1)} all-gather(bf16[256,256]{1,0:T(8,128)(2,1)S(1)} %concatenate.50), channel_id=1, replica_groups=mesh['grp'=2,'sp'=4,'tp'=4] {'sp'}, dimensions={0}, use_global_device_ids=true | all-gather | bytes 655360 | tf_op jit(solution)/shard_map/all_gather | solution.py:160
  29.0 1.1 copy.88
  30.8 0.6 bitcast_reduce_fusion.1
  31.5 1.3 copy-done.2
  33.2 14.7 %all_gather.14 = bf16[1024,128]{0,1:T(8,128)(2,1)S(1)} all-gather(bf16[256,128]{0,1:T(8,128)(2,1)S(1)} %copy.90), channel_id=1, replica_groups=mesh['grp'=2,'sp'=4,'tp'=4] {'sp'}, dimensions={0}, use_global_device_ids=true | all-gather | bytes 327680 | tf_op jit(solution)/shard_map/all_gather | solution.py:164
  48.5 13.8 %all_gather.12 = bf16[1024,128]{0,1:T(8,128)(2,1)S(1)} all-gather(bf16[256,128]{0,1:T(8,128)(2,1)S(1)} %bitcast.168), channel_id=1, replica_groups=mesh['grp'=2,'sp'=4,'tp'=4] {'sp'}, dimensions={0}, use_global_device_ids=true | all-gather | bytes 327680 | tf_op jit(solution)/shard_map/all_gather | solution.py:158
  62.6 0.8 bitcast_reduce_fusion
  63.4 0.7 fusion.1
  64.1 1.2 copy-done.1
  65.5 3.1 %fusion.38 = bf16[256,2,2,64]{0,3,2,1:T(8,128)(2,1)S(1)} fusion(bf16[1024,2,64,1]{0,2,3,1:T(8,128)(2,1)S(1)} %bitcast.166, f32[2,1024,256,2]{2,1,3,0:T(8,128)} %copy-done.1, f32[256,2,2]{0,2,1:T(2,128)S(1)} %broadcast_maximum_fusion, f32[256,2,2]{0,2,1:T(2,128)S(1)} %get-tuple-element.30, f32[256,2,2]{0,2,1:T(2,128)S(1)} %get-tuple-element.29), kind=kOutput, calls=%fused_computation.32 | convolution fusion | flops 137560064 | bytes 4599808 | tf_op jit(solution)/shard_map/qgrk,kgd->qgrd/dot_general | solution.py:77
  69.1 1.1 copy-done.3
  70.7 1.5 fusion.3
  73.3 25.2 %reduce-scatter.5.cloned.1.call-done = bf16[64,2048]{1,0:T(8,128)(2,1)} async-done(((bf16[256,2048]{1,0:T(8,128)(2,1)}), bf16[64,2048]{1,0:T(8,128)(2,1)}) %reduce-scatter.5.cloned.1.call-update) | async-done | bytes 262160 | tf_op jit(solution)/shard_map/reduce_scatter | solution.py:169
  98.5 1.1 fusion.48
  99.6 1.4 convolution_convert_fusion
  101.1 29.9 %all_to_all.10 = bf16[4,2,32,2048]{3,2,1,0:T(8,128)(2,1)S(1)} all-to-all(bf16[4,2,32,2048]{3,2,1,0:T(8,128)(2,1)S(1)} %bitcast.163), channel_id=1, replica_groups=mesh['grp'=2,'sp'=4,'tp'=4] {'sp'}, dimensions={0} | all-to-all | bytes 2097152 | tf_op jit(solution)/shard_map/all_to_all | solution.py:206
  131.0 1.0 copy.94
  132.3 32.5 %all-gather.2.cloned.1.call-done = bf16[16,2,32,2048]{3,2,0,1:T(8,128)(2,1)} async-done(((bf16[4,2,32,2048]{3,2,0,1:T(8,128)(2,1)}), bf16[16,2,32,2048]{3,2,0,1:T(8,128)(2,1)}) %all-gather.2.cloned.1.call-update) | async-done | bytes 4194320 | tf_op jit(solution)/shard_map/all_gather | solution.py:205
  164.8 4.1 %fusion.14 = f32[16,2,32,256]{3,2,0,1:T(8,128)S(1)} fusion(bf16[16,2,32,2048]{3,2,0,1:T(8,128)(2,1)} %all-gather.2.cloned.1.call-done, bf16[2,2048,256]{2,1,0:T(8,128)(2,1)} %param.35), kind=kOutput, calls=%fused_computation.21 | convolution fusion | flops 1073741824 | bytes 7340032 | tf_op jit(solution)/shard_map/secd,edf->secf/dot_general | solution.py:211
  169.0 7.3 %convert_bitcast_fusion = bf16[16,2,32,2048]{3,2,0,1:T(8,128)(2,1)} fusion(bf16[2,256,2048]{2,1,0:T(8,128)(2,1)S(1)} %copy-done, bf16[16,2,32,2048]{3,2,0,1:T(8,128)(2,1)} %all-gather.2.cloned.1.call-done, bf16[2,2048,256]{2,1,0:T(8,128)(2,1)} %param.36, f32[16,2,32,256]{3,2,0,1:T(8,128)S(1)} %fusion.14), kind=kOutput, calls=%fused_computation.3 | convolution fusion | flops 2151153664 | bytes 13631488 | tf_op jit(solution)/shard_map/secf,efd->secd/dot_general | solution.py:217
  176.3 0.6 copy-done.18
  176.9 0.6 dynamic-slice
  178.2 83.8 %all-reduce.3.cloned.1.call-done = bf16[16,2,32,2048]{3,2,0,1:T(8,128)(2,1)} async-done(((bf16[16,2,32,2048]{3,2,0,1:T(8,128)(2,1)}), bf16[16,2,32,2048]{3,2,0,1:T(8,128)(2,1)}) %all-reduce.3.cloned.1.call-update) | async-done | bytes 4194320
  261.9 1.3 constant_dynamic-slice_fusion
  263.3 1.1 copy.95
  264.3 4.6 %all-to-all-start.1 = ((bf16[4,2,32,2048]{3,2,1,0:T(8,128)(2,1)}), bf16[4,2,32,2048]{3,2,1,0:T(8,128)(2,1)S(1)}, u32[]{:S(2)}, u32[]{:S(2)}) async-start(bf16[4,2,32,2048]{3,2,1,0:T(8,128)(2,1)} %copy.95), calls=%async_computation.2 | async-start | bytes 2097152 | tf_op jit(solution)/shard_map/all_to_all | solution.py:224
  268.9 25.4 %all-to-all-done.1 = bf16[4,2,32,2048]{3,2,1,0:T(8,128)(2,1)S(1)} async-done(((bf16[4,2,32,2048]{3,2,1,0:T(8,128)(2,1)}), bf16[4,2,32,2048]{3,2,1,0:T(8,128)(2,1)S(1)}, u32[]{:S(2)}, u32[]{:S(2)}) %all-to-all-start.1) | async-done | bytes 1048608 | tf_op jit(solution)/shard_map/all_to_all | solution.py:224
  294.7 1.7 fusion.51
  (91 shorter events, 6.1 us)
Async XLA Ops:
  6.5 162.4 %copy-start = (bf16[2,256,2048]{2,1,0:T(8,128)(2,1)S(1)}, bf16[2,256,2048]{2,1,0:T(8,128)(2,1)}, u32[]{:S(2)}) copy-start(bf16[2,256,2048]{2,1,0:T(8,128)(2,1)} %param.37) | copy-start | bytes 6291460
  6.5 23.8 %copy-start.14 = (f32[128]{0:T(128)S(1)}, f32[128]{0:T(128)}, u32[]{:S(2)}) copy-start(f32[128]{0:T(128)} %param.27) | copy-start | bytes 1540
  6.5 91.9 %reduce-scatter.5.cloned.1.call-start = ((), (), s32[]{:S(2)}) async-start(), calls=%async_computation.3 | async-start | bytes 1310720 | tf_op jit(solution)/shard_map/reduce_scatter | solution.py:169
  29.0 2.4 copy-start.5
  30.8 2.4 copy-start.9
  30.8 17.2 %copy-start.17 = (f32[16]{0:T(128)S(1)}, f32[16]{0:T(128)}, u32[]{:S(2)}) copy-start(f32[16]{0:T(128)} %multiply_power_fusion.1) | copy-start | bytes 196
  30.8 17.4 %copy-start.10 = (bf16[256,128]{1,0:T(8,128)(2,1)S(1)}, bf16[256,128]{1,0:T(8,128)(2,1)}, u32[]{:S(2)}) copy-start(bf16[256,128]{1,0:T(8,128)(2,1)} %param.20) | copy-start | bytes 196612
  31.4 1.3 copy-start.2
  31.4 16.9 %copy-start.15 = (f32[64]{0:T(128)S(1)}, f32[64]{0:T(128)}, u32[]{:S(2)}) copy-start(f32[64]{0:T(128)} %param.26) | copy-start | bytes 772
  31.4 30.8 %copy-start.8 = (bf16[256,256]{1,0:T(8,128)(2,1)S(1)}, bf16[256,256]{1,0:T(8,128)(2,1)}, u32[]{:S(2)}) copy-start(bf16[256,256]{1,0:T(8,128)(2,1)} %param.19) | copy-start | bytes 393220
  31.5 31.0 %copy-start.16 = (f32[64]{0:T(128)S(1)}, f32[64]{0:T(128)}, u32[]{:S(2)}) copy-start(f32[64]{0:T(128)} %param.25) | copy-start | bytes 772
  63.4 1.9 copy-start.1
  63.4 1.9 slice-start
  65.5 3.1 %copy-start.6 = (bf16[256,2048]{1,0:T(8,128)(2,1)S(1)}, bf16[256,2048]{1,0:T(8,128)(2,1)}, u32[]{:S(2)}) copy-start(bf16[256,2048]{1,0:T(8,128)(2,1)} %param.30) | copy-start | bytes 3145732
  68.6 1.6 copy-start.3
  69.0 1.6 copy-start.7
  70.7 1.6 copy-start.12
  70.7 27.8 %copy-start.4 = (bf16[64,2048]{1,0:T(8,128)(2,1)S(1)}, bf16[64,2048]{1,0:T(8,128)(2,1)}, u32[]{:S(2)}) copy-start(bf16[64,2048]{1,0:T(8,128)(2,1)} %param.29) | copy-start | bytes 786436
  70.7 28.9 %copy-start.11 = (f32[2048]{0:T(1024)S(1)}, f32[2048]{0:T(1024)}, u32[]{:S(2)}) copy-start(f32[2048]{0:T(1024)} %param.32) | copy-start | bytes 24580
  72.2 92.6 %all-gather.2.cloned.1.call-start = ((), (), s32[]{:S(2)}) async-start(), calls=%async_computation.4 | async-start | bytes 5242880 | tf_op jit(solution)/shard_map/all_gather | solution.py:205
  132.1 129.9 %all-reduce.3.cloned.1.call-start = ((), (), s32[]{:S(2)}) async-start(), calls=%async_computation.5 | async-start | bytes 8388608
  176.3 0.7 copy-start.18
  263.2 5.7 %copy-start.13 = (f32[64,2]{0,1:T(2,128)S(1)}, f32[64,2]{0,1:T(2,128)}, u32[]{:S(2)}) copy-start(f32[64,2]{0,1:T(2,128)} %param.34) | copy-start | bytes 1540
  264.3 30.0 %all-to-all-start.1 = ((bf16[4,2,32,2048]{3,2,1,0:T(8,128)(2,1)}), bf16[4,2,32,2048]{3,2,1,0:T(8,128)(2,1)S(1)}, u32[]{:S(2)}, u32[]{:S(2)}) async-start(bf16[4,2,32,2048]{3,2,1,0:T(8,128)(2,1)} %copy.95), calls=%async_computation.2 | async-start | bytes 2097152 | tf_op jit(solution)/shard_map/all_to_all | solution.py:224
Sparse Core Ops, SparseCore 0:
  72.3 26.0 reduce-scatter.4
  132.2 32.5 all-gather.1
  176.4 85.4 all-reduce.2
